TPU v7x, 32 devices: a whole 2x2x4 slice. The times are simulated.
32 devices in a mesh: ep: 8 (over z, core), tp: 4 (over y, x).
Axes of the slice: x: 2, y: 2, z: 4, core: 2. Of those that a mesh axis runs over, the one named last changes fastest.
Arguments:
- tokens: bfloat16 [1024, 2048], P('ep'), may hold values from -6 to 6
- selected: int32 [8, 256], P(None, 'ep'), may hold values from -1 to 127, as said below
- affinity: float32 [8, 256], P(None, 'ep'), may hold values from 0.05 to 1
- w_gate: bfloat16 [8, 2048, 2048], P('ep', None, 'tp'), may hold values from -0.125 to 0.125
- w_up: bfloat16 [8, 2048, 2048], P('ep', None, 'tp'), may hold values from -0.125 to 0.125
- w_down: bfloat16 [8, 2048, 2048], P('ep', 'tp'), may hold values from -0.125 to 0.125
Outputs:
- combined: bfloat16 [1024, 2048], P('ep', 'tp')
Inputs may be any that keep to these rules, and one draw needn't show every extreme that they name: `selected`: row e holds 8 aligned groups of 32 entries; the live entries of group j are distinct positions within the j-th block of 128 tokens, stand at the front of the group and are followed by -1; each row has 128 live entries in all, the number in a group varies, and some group of every row is full.
All inputs are finite; a program needn't handle non-finite values.
Results may differ from a plain program's by a relative error of at most 0.015.
Values may be sent and summed in bfloat16 or wider, within the bound.
A program may use at most 64 MiB of HBM per device.

v0:
```python
import jax
import jax.numpy as jnp
from jax import lax
from jax.sharding import PartitionSpec as P


def per_device(tokens, selected, affinity, w_gate, w_up, w_down):
    ep_count = lax.axis_size("ep")
    local_tokens = tokens.shape[0]
    experts_here = w_gate.shape[0]
    slot_count = selected.shape[1]
    clamped = jnp.maximum(selected, 0)
    gathered = jnp.take(tokens, clamped, axis=0)
    arrived = lax.all_to_all(gathered, "ep", split_axis=0, concat_axis=1, tiled=True)
    gate_act = jnp.einsum("ecd,edf->ecf", arrived, w_gate, preferred_element_type=jnp.float32)
    up_act = jnp.einsum("ecd,edf->ecf", arrived, w_up, preferred_element_type=jnp.float32)
    hidden = (jax.nn.silu(gate_act) * up_act).astype(jnp.bfloat16)
    summed = lax.psum_scatter(
        jnp.einsum("efd,ecf->dec", w_down, hidden, preferred_element_type=jnp.float32).astype(
            jnp.bfloat16
        ),
        "tp",
        scatter_dimension=0,
        tiled=True,
    )
    summed = summed.reshape(summed.shape[0], experts_here, ep_count, slot_count)
    returned = lax.all_to_all(summed, "ep", split_axis=2, concat_axis=1, tiled=True)
    feature_cols = returned.shape[0]
    returned = returned.reshape(feature_cols, experts_here * ep_count * slot_count)
    weights = jnp.where(selected >= 0, affinity, jnp.zeros_like(affinity)).reshape(-1)
    scaled_rows = returned.astype(jnp.float32).T * weights[:, None]
    combined = (
        jnp.zeros((local_tokens, feature_cols), jnp.float32)
        .at[clamped.reshape(-1)]
        .add(scaled_rows)
    )
    return combined.astype(jnp.bfloat16)


def solution(mesh):
    placed = (
        P("ep", None),
        P(None, "ep"),
        P(None, "ep"),
        P("ep", None, "tp"),
        P("ep", None, "tp"),
        P("ep", "tp", None),
    )
    return jax.shard_map(
        per_device, mesh=mesh, in_specs=placed, out_specs=P("ep", "tp"), check_vma=False
    )
```

profile of v0, /device:TPU:0, one launch (start us, length us, event | category | flops | bytes accessed | tf_op | source)
XLA Modules:
  0.0 101.5 jit_solution(7033173364249277879)
XLA Ops:
  6.5 0.0 copy-start
  6.5 0.0 reduce-scatter.2.cloned.1.call-start
  6.5 0.8 broadcast_maximum_fusion
  7.4 0.7 broadcast_compare_fusion
  8.1 0.1 reshape.87
  8.2 3.5 %gather_fusion = bf16[256,2048]{1,0:T(8,128)(2,1)S(1)} fusion(bf16[128,2048]{1,0:T(8,128)(2,1)} %param.6, s32[1024]{0:T(1024)S(1)} %pad_clamp_fusion), kind=kCustom, calls=%fused_computation | custom fusion | bytes 2098176 | tf_op jit(solution)/shard_map/jit(_take)/gather | solution.py:13
  11.6 0.0 copy-start.3
  11.6 0.2 broadcast_select_fusion
  11.8 32.8 %all_to_all.8 = bf16[8,32,2048]{2,1,0:T(8,128)(2,1)S(1)} all-to-all(bf16[8,32,2048]{2,1,0:T(8,128)(2,1)S(1)} %broadcast_select_fusion), channel_id=1, replica_groups=mesh['ep'=8,'tp'=4] {'ep'}, dimensions={0} | all-to-all | bytes 2097152 | tf_op jit(solution)/shard_map/all_to_all | solution.py:14
  44.7 0.0 copy-done.3
  44.7 1.6 %fusion.4 = f32[256,512]{1,0:T(8,128)} fusion(bf16[256,2048]{1,0:T(8,128)(2,1)S(1)} %bitcast.34, bf16[1,2048,512]{2,1,0:T(8,128)(2,1)S(1)} %copy-done.3), kind=kOutput, calls=%fused_computation.7 | convolution fusion | flops 536870912 | bytes 3670016 | tf_op jit(solution)/shard_map/ecd,edf->ecf/dot_general | solution.py:15
  46.2 0.0 copy-done
  46.2 0.0 copy-start.1
  46.2 4.0 %fusion = bf16[2048,1,256]{0,2,1:T(8,128)(2,1)} fusion(bf16[1,512,2048]{2,1,0:T(8,128)(2,1)S(1)} %copy-done, bf16[256,2048]{1,0:T(8,128)(2,1)S(1)} %bitcast.35, bf16[1,2048,512]{2,1,0:T(8,128)(2,1)} %param.10, f32[256,512]{1,0:T(8,128)} %fusion.4), kind=kOutput, calls=%fused_computation.3 | convolution fusion | flops 1075052544 | bytes 6815744 | tf_op jit(solution)/shard_map/efd,ecf->dec/dot_general | solution.py:19
  50.3 0.0 reduce-scatter.2.cloned.1.call-update
  50.3 27.0 %reduce-scatter.2.cloned.1.call-done = bf16[512,1,256]{0,2,1:T(8,128)(2,1)} async-done(((bf16[2048,1,256]{0,2,1:T(8,128)(2,1)}), bf16[512,1,256]{0,2,1:T(8,128)(2,1)}) %reduce-scatter.2.cloned.1.call-update) | async-done | bytes 262160 | tf_op jit(solution)/shard_map/reduce_scatter | solution.py:18
  77.3 4.6 %all-to-all-start.1 = ((bf16[512,1,8,32]{0,3,1,2:T(8,128)(2,1)}), bf16[512,1,8,32]{0,3,1,2:T(8,128)(2,1)S(1)}, u32[]{:S(2)}, u32[]{:S(2)}) async-start(bf16[512,1,8,32]{0,3,1,2:T(8,128)(2,1)} %bitcast.36), calls=%async_computation.2 | async-start | bytes 524288 | tf_op jit(solution)/shard_map/all_to_all | solution.py:27
  81.9 0.1 reshape.78
  82.0 0.0 copy-done.1
  82.0 0.0 copy-done.2
  82.0 0.1 mul.24
  82.1 9.5 %all-to-all-done.1 = bf16[512,1,8,32]{0,3,1,2:T(8,128)(2,1)S(1)} async-done(((bf16[512,1,8,32]{0,3,1,2:T(8,128)(2,1)}), bf16[512,1,8,32]{0,3,1,2:T(8,128)(2,1)S(1)}, u32[]{:S(2)}, u32[]{:S(2)}) %all-to-all-start.1) | async-done | bytes 262176 | tf_op jit(solution)/shard_map/all_to_all | solution.py:27
  91.6 2.4 %scatter_custom_fusion = f32[128,512]{1,0:T(8,128)S(1)} fusion(s32[256]{0:T(256)S(1)} %bitcast.37, bf16[512,256]{0,1:T(8,128)(2,1)S(1)} %bitcast.33, f32[256]{0:T(256)S(1)} %mul.24, f32[]{:T(128)} %constant.9.clone.1), kind=kCustom, calls=%fused_computation.14 | custom fusion | flops 393216 | bytes 525316 | tf_op jit(solution)/shard_map/scatter-add | solution.py:35
  94.0 0.7 convert_element_type.28
  (4 shorter events, 0.0 us)
Async XLA Ops:
  6.5 39.7 %copy-start = (bf16[1,512,2048]{2,1,0:T(8,128)(2,1)S(1)}, bf16[1,512,2048]{2,1,0:T(8,128)(2,1)}, u32[]{:S(2)}) copy-start(bf16[1,512,2048]{2,1,0:T(8,128)(2,1)} %param.11) | copy-start | bytes 6291460
  6.5 70.8 %reduce-scatter.2.cloned.1.call-start = ((), (), s32[]{:S(2)}) async-start(), calls=%async_computation.3 | async-start | bytes 1310720 | tf_op jit(solution)/shard_map/reduce_scatter | solution.py:18
  11.6 33.0 %copy-start.3 = (bf16[1,2048,512]{2,1,0:T(8,128)(2,1)S(1)}, bf16[1,2048,512]{2,1,0:T(8,128)(2,1)}, u32[]{:S(2)}) copy-start(bf16[1,2048,512]{2,1,0:T(8,128)(2,1)} %param.9) | copy-start | bytes 6291460
  46.2 35.8 %copy-start.1 = (s32[8,32]{1,0:T(8,128)S(1)}, s32[8,32]{1,0:T(8,128)}, u32[]{:S(2)}) copy-start(s32[8,32]{1,0:T(8,128)} %param.7) | copy-start | bytes 3076
  46.2 35.8 %copy-start.2 = (f32[8,32]{1,0:T(8,128)S(1)}, f32[8,32]{1,0:T(8,128)}, u32[]{:S(2)}) copy-start(f32[8,32]{1,0:T(8,128)} %param.8) | copy-start | bytes 3076
  77.3 14.3 %all-to-all-start.1 = ((bf16[512,1,8,32]{0,3,1,2:T(8,128)(2,1)}), bf16[512,1,8,32]{0,3,1,2:T(8,128)(2,1)S(1)}, u32[]{:S(2)}, u32[]{:S(2)}) async-start(bf16[512,1,8,32]{0,3,1,2:T(8,128)(2,1)} %bitcast.36), calls=%async_computation.2 | async-start | bytes 524288 | tf_op jit(solution)/shard_map/all_to_all | solution.py:27
Sparse Core Ops, SparseCore 0:
  50.4 26.8 reduce-scatter.1
where the time goes:
time: 102 us
  waiting for transfers between devices  36.6 us (36%)
  blocking collectives  32.8 us (32%)
  between operations  13.4 us (13%)
  matrix products  5.59 us (5%)
  other arithmetic  4.75 us (5%)
  starting transfers between devices  4.62 us (5%)
  local copies, waits for them, and re-layouts  3.73 us (4%)
    all_to_all x1, blocking collectives, per_device(): lax.all_to_all(gathered, 'ep', split_axis=0, concat_axis=1, tiled=True)  32.8 us
    reduce_scatter x1, waiting for transfers between devices, per_device(): lax.psum_scatter(jnp.einsum('efd,ecf->dec', w_down, hidden, preferred_ele...  27 us
    all_to_all x1, waiting for transfers between devices, per_device(): lax.all_to_all(summed, 'ep', split_axis=2, concat_axis=1, tiled=True)  9.54 us
    all_to_all x1, starting transfers between devices, per_device(): lax.all_to_all(summed, 'ep', split_axis=2, concat_axis=1, tiled=True)  4.61 us
    dot_general x1, matrix products, per_device(): jnp.einsum('efd,ecf->dec', w_down, hidden, preferred_element_type=jnp.flo...  4.04 us
    gather x1, local copies, waits for them, and re-layouts, per_device(): gathered = jnp.take(tokens, clamped, axis=0)  3.48 us
    scatter-add x1, other arithmetic, per_device(): combined = jnp.zeros((local_tokens, feature_cols), jnp.float32).at[clampe...  2.37 us
  transfers between devices with their start and end apart: 2, of which 2 were waited for; matrix products, arithmetic and copies ran while one was open for 0% of the time, Pallas kernels for 0%

commit v1 on v0

--- a/solution.py
+++ b/solution.py
@@ -24,7 +24,10 @@
         tiled=True,
     )
     summed = summed.reshape(summed.shape[0], experts_here, ep_count, slot_count)
-    returned = lax.all_to_all(summed, "ep", split_axis=2, concat_axis=1, tiled=True)
+    returned = jnp.concatenate(
+        lax.all_to_all(jnp.stack(jnp.split(summed, lax.axis_size("ep"), axis=2)), "ep", 0, 0),
+        axis=1,
+    )
     feature_cols = returned.shape[0]
     returned = returned.reshape(feature_cols, experts_here * ep_count * slot_count)
     weights = jnp.where(selected >= 0, affinity, jnp.zeros_like(affinity)).reshape(-1)

time: 102 us -> 113 us (1.11)
  local copies, waits for them, and re-layouts: 3.73 us -> 14.6 us
    unnamed x8 -> x15, local copies, waits for them, and re-layouts: 0.02 us -> 9.55 us
    another operation x0 -> x1, local copies, waits for them, and re-layouts: none -> 1.36 us  [per_device(): jnp.stack(jnp.split(summed, lax.axis_size('ep'), axis=2))]
where the time goes in v1:
time: 113 us; the launch traced here: 112 us
  waiting for transfers between devices  36.6 us (32%)
  blocking collectives  32.8 us (29%)
  local copies, waits for them, and re-layouts  14.6 us (13%)
  between operations  13.4 us (12%)
  matrix products  5.57 us (5%)
  other arithmetic  4.79 us (4%)
  starting transfers between devices  4.6 us (4%)
    all_to_all x1, blocking collectives, per_device(): lax.all_to_all(gathered, 'ep', split_axis=0, concat_axis=1, tiled=True)  32.8 us
    reduce_scatter x1, waiting for transfers between devices, per_device(): lax.psum_scatter(jnp.einsum('efd,ecf->dec', w_down, hidden, preferred_ele...  27 us
    unnamed x15, local copies, waits for them, and re-layouts  9.55 us
    all_to_all x1, waiting for transfers between devices, per_device(): lax.all_to_all(jnp.stack(jnp.split(summed, lax.axis_size('ep'), axis=2)),...  9.54 us
    all_to_all x1, starting transfers between devices, per_device(): lax.all_to_all(jnp.stack(jnp.split(summed, lax.axis_size('ep'), axis=2)),...  4.6 us
    dot_general x1, matrix products, per_device(): jnp.einsum('efd,ecf->dec', w_down, hidden, preferred_element_type=jnp.flo...  4.03 us
    gather x1, local copies, waits for them, and re-layouts, per_device(): gathered = jnp.take(tokens, clamped, axis=0)  3.48 us
    scatter-add x1, other arithmetic, per_device(): combined = jnp.zeros((local_tokens, feature_cols), jnp.float32).at[clampe...  2.31 us
  transfers between devices with their start and end apart: 2, of which 2 were waited for; matrix products, arithmetic and copies ran while one was open for 0% of the time, Pallas kernels for 0%

profile of v1, /device:TPU:0, one launch (start us, length us, event | category | flops | bytes accessed | tf_op | source)
XLA Modules:
  0.0 112.4 jit_solution(15528485477544004841)
XLA Ops:
  6.5 0.8 broadcast_compare_fusion
  7.4 0.7 broadcast_maximum_fusion
  8.1 0.1 reshape.83
  8.2 3.5 %gather_fusion = bf16[256,2048]{1,0:T(8,128)(2,1)S(1)} fusion(bf16[128,2048]{1,0:T(8,128)(2,1)} %param.6, s32[1024]{0:T(1024)S(1)} %pad_clamp_fusion), kind=kCustom, calls=%fused_computation | custom fusion | bytes 2098176 | tf_op jit(solution)/shard_map/jit(_take)/gather | solution.py:13
  11.7 0.2 broadcast_select_fusion
  11.8 32.8 %all_to_all.14 = bf16[8,32,2048]{2,1,0:T(8,128)(2,1)S(1)} all-to-all(bf16[8,32,2048]{2,1,0:T(8,128)(2,1)S(1)} %broadcast_select_fusion), channel_id=1, replica_groups=mesh['ep'=8,'tp'=4] {'ep'}, dimensions={0} | all-to-all | bytes 2097152 | tf_op jit(solution)/shard_map/all_to_all | solution.py:14
  44.7 1.5 %fusion.4 = f32[256,512]{1,0:T(8,128)} fusion(bf16[256,2048]{1,0:T(8,128)(2,1)S(1)} %bitcast.65, bf16[1,2048,512]{2,1,0:T(8,128)(2,1)S(1)} %copy-done.3), kind=kOutput, calls=%fused_computation.7 | convolution fusion | flops 536870912 | bytes 3670016 | tf_op jit(solution)/shard_map/ecd,edf->ecf/dot_general | solution.py:15
  46.2 4.0 %fusion = bf16[2048,1,256]{0,2,1:T(8,128)(2,1)} fusion(bf16[1,512,2048]{2,1,0:T(8,128)(2,1)S(1)} %copy-done, bf16[256,2048]{1,0:T(8,128)(2,1)S(1)} %bitcast.66, bf16[1,2048,512]{2,1,0:T(8,128)(2,1)} %param.10, f32[256,512]{1,0:T(8,128)} %fusion.4), kind=kOutput, calls=%fused_computation.3 | convolution fusion | flops 1075052544 | bytes 6815744 | tf_op jit(solution)/shard_map/efd,ecf->dec/dot_general | solution.py:19
  50.3 27.0 %reduce-scatter.2.cloned.1.call-done = bf16[512,1,256]{0,2,1:T(8,128)(2,1)} async-done(((bf16[2048,1,256]{0,2,1:T(8,128)(2,1)}), bf16[512,1,256]{0,2,1:T(8,128)(2,1)}) %reduce-scatter.2.cloned.1.call-update) | async-done | bytes 262160 | tf_op jit(solution)/shard_map/reduce_scatter | solution.py:18
  77.3 1.4 %fusion.30 = bf16[8,512,1,1,32]{1,4,3,2,0:T(8,128)(2,1)} fusion(bf16[512,1,8,32]{0,3,2,1:T(8,128)(2,1)} %bitcast.67), kind=kLoop, calls=%fused_computation.37 | loop fusion | bytes 65536
  78.7 1.4 %fusion.29 = bf16[8,512,1,1,32]{1,4,3,2,0:T(8,128)(2,1)} fusion(bf16[8,512,1,1,32]{1,4,3,2,0:T(8,128)(2,1)} %fusion.30, bf16[512,1,8,32]{0,3,2,1:T(8,128)(2,1)} %bitcast.68), kind=kLoop, calls=%fused_computation.35 | loop fusion | bytes 65536
  80.0 1.4 %fusion.28 = bf16[8,512,1,1,32]{1,4,3,2,0:T(8,128)(2,1)} fusion(bf16[8,512,1,1,32]{1,4,3,2,0:T(8,128)(2,1)} %fusion.29, bf16[512,1,8,32]{0,3,2,1:T(8,128)(2,1)} %bitcast.69), kind=kLoop, calls=%fused_computation.33 | loop fusion | bytes 65536
  81.4 1.4 %fusion.27 = bf16[8,512,1,1,32]{1,4,3,2,0:T(8,128)(2,1)} fusion(bf16[8,512,1,1,32]{1,4,3,2,0:T(8,128)(2,1)} %fusion.28, bf16[512,1,8,32]{0,3,2,1:T(8,128)(2,1)} %bitcast.70), kind=kLoop, calls=%fused_computation.31 | loop fusion | bytes 65536
  82.7 1.4 %fusion.26 = bf16[8,512,1,1,32]{1,4,3,2,0:T(8,128)(2,1)} fusion(bf16[8,512,1,1,32]{1,4,3,2,0:T(8,128)(2,1)} %fusion.27, bf16[512,1,8,32]{0,3,2,1:T(8,128)(2,1)} %bitcast.71), kind=kLoop, calls=%fused_computation.29 | loop fusion | bytes 65536
  84.1 1.4 %fusion.25 = bf16[8,512,1,1,32]{1,4,3,2,0:T(8,128)(2,1)} fusion(bf16[8,512,1,1,32]{1,4,3,2,0:T(8,128)(2,1)} %fusion.26, bf16[512,1,8,32]{0,3,2,1:T(8,128)(2,1)} %bitcast.72), kind=kLoop, calls=%fused_computation.27 | loop fusion | bytes 65536
  85.5 1.4 %fusion.24 = bf16[8,512,1,1,32]{1,4,3,2,0:T(8,128)(2,1)} fusion(bf16[8,512,1,1,32]{1,4,3,2,0:T(8,128)(2,1)} %fusion.25, bf16[512,1,8,32]{0,3,2,1:T(8,128)(2,1)} %bitcast.73), kind=kLoop, calls=%fused_computation.25 | loop fusion | bytes 65536
  86.8 1.4 %fusion.23 = bf16[8,512,1,1,32]{1,4,3,2,0:T(8,128)(2,1)} fusion(bf16[8,512,1,1,32]{1,4,3,2,0:T(8,128)(2,1)} %fusion.24, bf16[512,1,8,32]{0,3,2,1:T(8,128)(2,1)} %bitcast.74), kind=kLoop, calls=%fused_computation.23 | loop fusion | bytes 65536 | tf_op jit(solution)/shard_map/stack | solution.py:28
  88.2 4.6 %all-to-all-start.1 = ((bf16[8,512,1,1,32]{1,4,3,2,0:T(8,128)(2,1)}), bf16[8,512,1,1,32]{1,4,3,2,0:T(8,128)(2,1)S(1)}, u32[]{:S(2)}, u32[]{:S(2)}) async-start(bf16[8,512,1,1,32]{1,4,3,2,0:T(8,128)(2,1)} %fusion.23), calls=%async_computation.2 | async-start | bytes 524288 | tf_op jit(solution)/shard_map/all_to_all | solution.py:28
  92.8 0.1 reshape.74
  92.9 0.1 mul.24
  93.0 9.5 %all-to-all-done.1 = bf16[8,512,1,1,32]{1,4,3,2,0:T(8,128)(2,1)S(1)} async-done(((bf16[8,512,1,1,32]{1,4,3,2,0:T(8,128)(2,1)}), bf16[8,512,1,1,32]{1,4,3,2,0:T(8,128)(2,1)S(1)}, u32[]{:S(2)}, u32[]{:S(2)}) %all-to-all-start.1) | async-done | bytes 262176 | tf_op jit(solution)/shard_map/all_to_all | solution.py:28
  102.5 0.1 bitcast_multiply_fusion
  102.6 2.3 %scatter_custom_fusion = f32[128,512]{1,0:T(8,128)S(1)} fusion(s32[256]{0:T(256)S(1)} %bitcast.75, f32[512,256]{0,1:T(8,128)S(1)} %bitcast_multiply_fusion, f32[]{:T(128)} %constant.9.clone.1), kind=kCustom, calls=%fused_computation.13 | custom fusion | flops 131072 | bytes 786436 | tf_op jit(solution)/shard_map/scatter-add | solution.py:38
  104.9 0.7 convert_element_type.32
  (13 shorter events, 0.1 us)
Async XLA Ops:
  6.5 39.7 %copy-start = (bf16[1,512,2048]{2,1,0:T(8,128)(2,1)S(1)}, bf16[1,512,2048]{2,1,0:T(8,128)(2,1)}, u32[]{:S(2)}) copy-start(bf16[1,512,2048]{2,1,0:T(8,128)(2,1)} %param.11) | copy-start | bytes 6291460
  6.5 70.8 %reduce-scatter.2.cloned.1.call-start = ((), (), s32[]{:S(2)}) async-start(), calls=%async_computation.3 | async-start | bytes 1310720 | tf_op jit(solution)/shard_map/reduce_scatter | solution.py:18
  11.6 33.0 %copy-start.3 = (bf16[1,2048,512]{2,1,0:T(8,128)(2,1)S(1)}, bf16[1,2048,512]{2,1,0:T(8,128)(2,1)}, u32[]{:S(2)}) copy-start(bf16[1,2048,512]{2,1,0:T(8,128)(2,1)} %param.9) | copy-start | bytes 6291460
  50.2 42.6 %copy-start.1 = (s32[8,32]{1,0:T(8,128)S(1)}, s32[8,32]{1,0:T(8,128)}, u32[]{:S(2)}) copy-start(s32[8,32]{1,0:T(8,128)} %param.7) | copy-start | bytes 3076
  50.3 42.6 %copy-start.2 = (f32[8,32]{1,0:T(8,128)S(1)}, f32[8,32]{1,0:T(8,128)}, u32[]{:S(2)}) copy-start(f32[8,32]{1,0:T(8,128)} %param.8) | copy-start | bytes 3076
  88.2 14.3 %all-to-all-start.1 = ((bf16[8,512,1,1,32]{1,4,3,2,0:T(8,128)(2,1)}), bf16[8,512,1,1,32]{1,4,3,2,0:T(8,128)(2,1)S(1)}, u32[]{:S(2)}, u32[]{:S(2)}) async-start(bf16[8,512,1,1,32]{1,4,3,2,0:T(8,128)(2,1)} %fusion.23), calls=%async_computation.2 | async-start | bytes 524288 | tf_op jit(solution)/shard_map/all_to_all | solution.py:28
Sparse Core Ops, SparseCore 0:
  50.4 26.8 reduce-scatter.1
